TPU v7x, 512 devices: a whole 4x8x8 slice. The times are simulated.
512 devices in a mesh: sp: 64 (over z, y), tp: 8 (over x, core).
Axes of the slice: x: 4, y: 8, z: 8, core: 2. Of those that a mesh axis runs over, the one named last changes fastest.
Arguments:
- tokens: bfloat16 [16384, 2048], P(('sp', 'tp')), may hold values from -6 to 6
- gain: float32 [2048], replicated, may hold values from 0.1 to 1.9
- w_ret_q: bfloat16 [2048, 2048], P(None, 'tp'), may hold values from -0.125 to 0.125
- w_ret_k: bfloat16 [2048, 2048], P(None, 'tp'), may hold values from -0.125 to 0.125
- w_ret_v: bfloat16 [2048, 2048], P(None, 'tp'), may hold values from -0.125 to 0.125
- w_fox_q: bfloat16 [2048, 1024], P(None, 'tp'), may hold values from -0.125 to 0.125
- w_fox_k: bfloat16 [2048, 1024], P(None, 'tp'), may hold values from -0.125 to 0.125
- w_fox_v: bfloat16 [2048, 1024], P(None, 'tp'), may hold values from -0.125 to 0.125
- fox_gates: float32 [16384, 8], P('sp', 'tp'), may hold values from -16384 to 0, as said below
- w_out_ret: bfloat16 [2048, 2048], P('tp', 'sp'), may hold values from -0.109375 to 0.109375
- w_out_fox: bfloat16 [1024, 2048], P('tp', 'sp'), may hold values from -0.109375 to 0.109375
Outputs:
- mixed: bfloat16 [16384, 2048], P(('sp', 'tp'))
Inputs may be any that keep to these rules, and one draw needn't show every extreme that they name: `fox_gates`: each head's values never rise along positions.
All inputs are finite; a program needn't handle non-finite values.
Results may differ from a plain program's by a relative error of at most 0.02.
Values may be sent and summed in bfloat16 or wider, within the bound.
No kernel may reach another device: no remote copies, remote signals or barrier semaphores. Data moves between devices by JAX's collectives and lax.ppermute only.
A program may use at most 128 MiB of HBM per device.

v0:
```python
import math
import jax
import jax.numpy as jnp
from jax import lax
from jax.sharding import Mesh
from jax.sharding import PartitionSpec as P

RET_HEADS = 8
RET_DIM = 256
FOX_DIM = 128
BLOCK = 128
SP = ("sp_0", "sp_1")
SP_TP = ("sp_0", "sp_1", "tp")
eps = 1e-06


def joined_along(pieces, dim):
    dims = list(pieces.shape[1:])
    dims[dim] *= pieces.shape[0]
    return jnp.moveaxis(pieces, 0, dim).reshape(dims)


def sent_to_all(shard, axis):
    size = lax.axis_size(axis)
    return lax.all_to_all(
        jnp.broadcast_to(shard[None], (size, *shard.shape)), axis, 0, 0, tiled=True
    )


def gathered_copies(shard, axis, dim):
    return joined_along(sent_to_all(shard, axis), dim)


def filled_with(shard, identity):
    return jax.tree.map(
        lambda part, zero: jnp.zeros_like(part) + jnp.asarray(zero, part.dtype), shard, identity
    )


def entering(shard, axes, combine, identity):
    before = start = filled_with(shard, identity)
    subtotal = shard
    for axis in reversed(axes):
        size, index = (lax.axis_size(axis), lax.axis_index(axis))
        pieces = jax.tree.map(lambda part: lax.all_gather(part, axis), subtotal)
        inside, subtotal = (start, start)
        for k in range(size):
            passed = k < index
            subtotal = combine(subtotal, jax.tree.map(lambda part: part[k], pieces))
            inside = jax.tree.map(lambda new, old: jnp.where(passed, new, old), subtotal, inside)
        before = combine(inside, before)
    return before


def side_by_side(arrays, axis, dim, along):
    widths = [a.shape[along] for a in arrays]
    both = jnp.concatenate(arrays, axis=along)
    out = lax.all_gather(both, axis, axis=dim, tiled=True)
    return tuple(jnp.split(out, [sum(widths[:k]) for k in range(1, len(widths))], axis=along))


def rows_first(arrays, axis, dims):
    turned = [jnp.moveaxis(a, dim, 0) for a, dim in zip(arrays, dims)]
    widths = [t[0].size for t in turned]
    both = jnp.concatenate([t.reshape(-1, w) for t, w in zip(turned, widths)], axis=1)
    out = lax.all_gather(both, axis, axis=0, tiled=True)
    pieces = jnp.split(out, [sum(widths[:k]) for k in range(1, len(widths))], axis=1)
    return tuple(
        (
            jnp.moveaxis(b.reshape(-1, *t.shape[1:]), 0, dim)
            for b, t, dim in zip(pieces, turned, dims)
        )
    )


def in_blocks(shard, dim, size):
    before, after = (shard.shape[:dim], shard.shape[dim + 1 :])
    return jnp.moveaxis(shard.reshape(*before, size, -1, *after), dim, 0)


def sent_and_summed(shard, axis, dim):
    size = lax.axis_size(axis)
    pieces = lax.all_to_all(in_blocks(shard, dim, size), axis, 0, 0, tiled=True)
    return jnp.sum(pieces.astype(jnp.float32), axis=0)


def head_norm(values, width):
    rows_here = values.shape[0]
    grouped = values.reshape(rows_here, -1, width)
    scaled = grouped * lax.rsqrt(jnp.mean(grouped * grouped, axis=2, keepdims=True) + eps)
    return scaled.reshape(rows_here, -1).astype(jnp.bfloat16)


def rotate(values, token_positions, width):
    rows_here = values.shape[0]
    half_width = width // 2
    inverse = 10000.0 ** (-jnp.arange(half_width, dtype=jnp.float32) / half_width)
    angles = token_positions.astype(jnp.float32)[:, None] * inverse[None, :]
    cosine = jnp.cos(angles)[:, None, :]
    sine = jnp.sin(angles)[:, None, :]
    grouped = values.astype(jnp.float32).reshape(rows_here, -1, width)
    first_half = grouped[..., :half_width]
    second_half = grouped[..., half_width:]
    turned = jnp.concatenate(
        [first_half * cosine - second_half * sine, first_half * sine + second_half * cosine],
        axis=-1,
    )
    return turned.reshape(rows_here, -1)


def decay_rates(head_ids, total):
    heads_float = head_ids.astype(jnp.float32)
    middle = RET_HEADS // 2
    fast_rate = 1.0 / (32.0 + 16.0 * heads_float)
    slow_rate = jnp.exp2(-(heads_float - middle)) / total
    return jnp.where(head_ids < middle, fast_rate, slow_rate)


def decay_tables(rates):
    offsets = jnp.arange(BLOCK, dtype=jnp.float32)
    spread = offsets[:, None] - offsets[None, :]
    causal = spread >= 0
    within = jnp.where(
        causal[None], jnp.exp(-rates[:, None, None] * jnp.where(causal, spread, 0.0)[None]), 0.0
    )
    query_decay = jnp.exp(-rates[None, :] * (offsets[:, None] + 1.0))
    key_decay = jnp.exp(-rates[None, :] * (BLOCK - 1.0 - offsets[:, None]))
    block_decay = jnp.exp(-rates * BLOCK)
    return (within, query_decay, key_decay, block_decay)


def advance(carry, key_block, value_block, key_decay, block_decay):
    scaled = (key_block.astype(jnp.float32) * key_decay[:, :, None]).astype(jnp.bfloat16)
    update = jnp.einsum("shd,she->hde", scaled, value_block, preferred_element_type=jnp.float32)
    return carry * block_decay[:, None, None] + update


def retention_blocks(queries, keys, values, rates, state, heads):
    within, query_decay, key_decay, block_decay = decay_tables(rates)
    count = queries.shape[0] // BLOCK

    def shaped(array):
        return array.reshape(count, BLOCK, heads, RET_DIM)

    def step(carry, blocks):
        query_block, key_block, value_block = blocks
        scores = (
            jnp.einsum("thd,shd->hts", query_block, key_block, preferred_element_type=jnp.float32)
            * within
        )
        inner = jnp.einsum(
            "hts,she->the",
            scores.astype(jnp.bfloat16),
            value_block,
            preferred_element_type=jnp.float32,
        )
        cross = (
            jnp.einsum("thd,hde->the", query_block.astype(jnp.float32), carry)
            * query_decay[:, :, None]
        )
        return (advance(carry, key_block, value_block, key_decay, block_decay), inner + cross)

    final_state, outputs = lax.scan(step, state, (shaped(queries), shaped(keys), shaped(values)))
    return (final_state, outputs.reshape(count * BLOCK, heads * RET_DIM))


def join_states(earlier, later):
    return (earlier[0] * later[0], earlier[1] * later[0][:, None, None] + later[1])


def fox_weights(queries, keys, query_gates, key_gates, query_pos, key_pos):
    scores = jnp.einsum(
        "qhd,khd->hqk", queries, keys, preferred_element_type=jnp.float32
    ) * FOX_DIM ** (-0.5)
    scores = scores + query_gates.T[:, :, None] - key_gates.T[:, None, :]
    allowed = key_pos[None, :] <= query_pos[:, None]
    return jnp.exp(jnp.where(allowed[None], scores, -jnp.inf))


def add_block(numer, denom, weights, values):
    numer = numer + jnp.einsum(
        "hqk,khd->qhd", weights.astype(jnp.bfloat16), values, preferred_element_type=jnp.float32
    )
    denom = denom + jnp.sum(weights, axis=2).T
    return (numer, denom)


def per_device(
    tokens,
    gain,
    w_ret_q,
    w_ret_k,
    w_ret_v,
    w_fox_q,
    w_fox_k,
    w_fox_v,
    fox_gates,
    w_out_ret,
    w_out_fox,
):
    inputs = tokens.astype(jnp.float32)
    normed = (
        inputs * lax.rsqrt(jnp.mean(inputs * inputs, axis=1, keepdims=True) + eps) * gain
    ).astype(jnp.bfloat16)
    weights_in = (w_ret_q, w_ret_k, w_ret_v, w_fox_q, w_fox_k, w_fox_v)
    piece = gathered_copies(normed, "tp", 0)
    products = [jnp.dot(piece, matrix, preferred_element_type=jnp.float32) for matrix in weights_in]
    projected = jnp.concatenate(products, axis=1).astype(jnp.bfloat16)
    ret_width = w_ret_q.shape[1]
    fox_width = w_fox_q.shape[1]
    edges = [
        0,
        ret_width,
        2 * ret_width,
        3 * ret_width,
        3 * ret_width + fox_width,
        3 * ret_width + 2 * fox_width,
        3 * ret_width + 3 * fox_width,
    ]
    pieces_out = [projected[:, edges[column] : edges[column + 1]] for column in range(6)]
    ret_query, ret_key, ret_value, fox_query, fox_key, fox_value = pieces_out
    length = projected.shape[0]
    sp_count = lax.axis_size(SP)
    total = length * sp_count
    offset = lax.axis_index(SP) * length
    token_positions = offset + jnp.arange(length, dtype=jnp.int32)
    ret_heads = ret_width // RET_DIM
    fox_heads = fox_width // FOX_DIM
    head_ids = lax.axis_index("tp") * ret_heads + jnp.arange(ret_heads, dtype=jnp.int32)
    rates = decay_rates(head_ids, float(total))
    query_rot = rotate(ret_query, token_positions, RET_DIM).astype(jnp.bfloat16)
    key_rot = (rotate(ret_key, token_positions, RET_DIM) * RET_DIM ** (-0.5)).astype(jnp.bfloat16)
    span_decay = jnp.exp(-rates * length)
    empty_state = jnp.zeros((ret_heads, RET_DIM, RET_DIM), jnp.float32)
    identity = (jnp.ones_like(span_decay), empty_state)
    final_state, local_part = retention_blocks(
        query_rot, key_rot, ret_value, rates, empty_state, ret_heads
    )
    carried = entering((span_decay, final_state), SP, join_states, identity)[1]
    query_up = query_rot.astype(jnp.float32).reshape(length, ret_heads, RET_DIM)
    steps_in = jnp.arange(length, dtype=jnp.float32)
    reach = jnp.exp(-rates[None, :] * (steps_in[:, None] + 1.0))
    carried_part = jnp.einsum("thd,hde->the", query_up, carried) * reach[:, :, None]
    ret_raw = local_part + carried_part.reshape(length, ret_width)
    ret_mixed = head_norm(ret_raw, RET_DIM)
    gates_all = gathered_copies(fox_gates, SP, 0)
    query3 = fox_query.reshape(length, fox_heads, FOX_DIM)
    zero_numer = jnp.zeros((length, fox_heads, FOX_DIM), jnp.float32)
    zero_denom = jnp.zeros((length, fox_heads), jnp.float32)
    last_query = offset + length - 1
    keys, values = side_by_side((fox_key, fox_value), SP, 0, 1)
    rows_here = keys.shape[0]
    width = math.gcd(rows_here, 512)

    def one_block(state, index):
        begin = index * width

        def compute(accum):
            key_block = lax.dynamic_slice_in_dim(keys, begin, width, 0).reshape(
                width, fox_heads, FOX_DIM
            )
            value_block = lax.dynamic_slice_in_dim(values, begin, width, 0).reshape(
                width, fox_heads, FOX_DIM
            )
            key_gates = lax.dynamic_slice_in_dim(gates_all, begin, width, 0)
            key_pos = begin + jnp.arange(width, dtype=jnp.int32)
            weights = fox_weights(query3, key_block, fox_gates, key_gates, token_positions, key_pos)
            return add_block(accum[0], accum[1], weights, value_block)

        def skip(accum):
            return accum

        return (lax.cond(begin <= last_query, compute, skip, state), None)

    result, _ = lax.scan(
        one_block, (zero_numer, zero_denom), jnp.arange(rows_here // width, dtype=jnp.int32)
    )
    numer, denom = result
    fox_raw = (numer / denom[:, :, None]).reshape(length, fox_width)
    fox_mixed = head_norm(fox_raw, FOX_DIM)
    out_ret, out_fox = rows_first((w_out_ret, w_out_fox), SP, (1, 1))
    summed = sent_and_summed(
        (
            jnp.dot(ret_mixed, out_ret, preferred_element_type=jnp.float32)
            + jnp.dot(fox_mixed, out_fox, preferred_element_type=jnp.float32)
        ).astype(jnp.bfloat16),
        "tp",
        0,
    )
    return summed.astype(jnp.bfloat16)


def solution(mesh):
    split = Mesh(mesh.devices.reshape(8, 8, mesh.shape["tp"]), ("sp_0", "sp_1", "tp"))
    return jax.shard_map(
        per_device,
        mesh=split,
        in_specs=(
            P(SP_TP, None),
            P(),
            P(None, "tp"),
            P(None, "tp"),
            P(None, "tp"),
            P(None, "tp"),
            P(None, "tp"),
            P(None, "tp"),
            P(SP, "tp"),
            P("tp", SP),
            P("tp", SP),
        ),
        out_specs=P(SP_TP, None),
        check_vma=False,
    )
```

profile of v0, /device:TPU:496, one launch (start us, length us, event | category | flops | bytes accessed | tf_op | source)
XLA Modules:
  0.0 491.8 jit_solution(2575343854345460355)
XLA Ops:
  9.8 4.3 all-to-all-start
  14.3 15.7 %all-to-all-done = bf16[8,32,2048]{2,1,0:T(8,128)(2,1)S(1)} async-done(((bf16[8,32,2048]{2,1,0:T(8,128)(2,1)}), bf16[8,32,2048]{2,1,0:T(8,128)(2,1)S(1)}, u32[]{:S(2)}, u32[]{:S(2)}) %all-to-all-start) | async-done | bytes 1048608 | tf_op jit(solution)/shard_map/all_to_all | solution.py:25
  33.7 7.6 %while.29 = (s32[]{:T(128)}, f32[1,256,256]{2,1,0:T(8,128)S(1)}, f32[2,128,1,256]{1,0,3,2:T(2,128)S(1)}, f32[1]{0:T(128)}, bf16[2,128,1,256]{3,1,2,0:T(8,128)(2,...) while((s32[]{:T(128)}, f32[1,256,256]{2,1,0:T(8,128)S(1)}, ...), condition=%wide.region_2.3_spmd.clone.clone.clone, body=%wide.region_1.2_spmd.clone.clone.clone.sunk | while | flops 50872832 | bytes 1840267 | solution.py:163
  34.3 2.9 dynamic_update_slice.8
  38.1 2.9 dynamic_update_slice.8
  44.1 14.3 %all-reduce = f32[8]{0:T(128)S(1)} all-reduce(f32[8]{0:T(128)S(1)} %dynamic-update-slice), channel_id=2, replica_groups=mesh['sp_0'=8,'sp_1'=8,'tp'=8] {'sp_1'}, use_global_device_ids=true, to_apply=%add | all-reduce | flops 8 | bytes 64
  60.9 20.0 %all-gather.14.cloned.1.call-done = f32[8,256,256]{2,1,0:T(8,128)} async-done(((f32[1,256,256]{2,1,0:T(8,128)}), f32[8,256,256]{2,1,0:T(8,128)}) %all-gather.14.cloned.1.call-update) | async-done | bytes 2097168 | tf_op jit(solution)/shard_map/all_gather | solution.py:45
  80.9 6.7 %bitcast_add_fusion.4 = f32[1,1,256,256]{3,2,1,0:T(8,128)} fusion(f32[8,256,256]{2,1,0:T(8,128)} %all-gather.14.cloned.1.call-done, f32[]{:T(128)} %bitcast.32, f32[]{:T(128)} %bitcast.30, f32[]{:T(128)} %bitcast.28, f32[]{:T(128)} %bitcast.26, f32[]{:T(128)} %bitcast.24, f32[]{:T(128)} %bitcast.23, f32[]{:T(128)} %bitcast.22, f32[]{:T(128)} %bitcast.21), kind=kLoop, calls=%fused_computation.120 | loop fusion | flops 983040 | bytes 2359328 | tf_op jit(solution)/shard_map/add | solution.py:168
  94.7 11.7 %all-to-all-start.1 = ((f32[64,256,1]{1,2,0:T(1,128)}), f32[64,256,1]{1,2,0:T(1,128)S(1)}, u32[]{:S(2)}, u32[]{:S(2)}) async-start(f32[64,256,1]{1,2,0:T(1,128)} %broadcast_in_dim.33), calls=%async_computation.1 | async-start | bytes 131072 | tf_op jit(solution)/shard_map/all_to_all | solution.py:25
  106.4 15.3 %all-reduce.1 = f32[8]{0:T(128)S(1)} all-reduce(f32[8]{0:T(128)S(1)} %dynamic-update-slice.1), channel_id=3, replica_groups=mesh['sp_0'=8,'sp_1'=8,'tp'=8] {'sp_0'}, use_global_device_ids=true, to_apply=%add.1 | all-reduce | flops 8 | bytes 64
  131.2 11.3 %multiply_reduce_fusion = (f32[256]{0:T(256)S(1)}, f32[256,1,256]{0,2,1:T(8,128)S(1)}) fusion(f32[256,1,256]{0,2,1:T(8,128)S(1)} %reshape.652, f32[256]{0:T(256)S(1)} %multiply_exponential_fusion, bf16[256,128]{0,1:T(8,128)(2,1)S(1)} %bitcast.300, bf16[256,128]{0,1:T(8,128)(2,1)S(1)} %bitcast.299, f32[8,1,256,256]{3,2,1,0:T(8,128)} %all-gather.8.cloned.1.call-done, ...), kind=kOutput, calls=%fused_computation.139 | convolution fusion | flops 37224192 | bytes 4851796 | tf_op jit(solution)/shard_map/thd,hde->the/dot_general | solution.py:243
  142.5 71.0 %all-gather.10.cloned.1.call-done = bf16[2048,384]{1,0:T(8,128)(2,1)} async-done(((bf16[32,384]{1,0:T(8,128)(2,1)}), bf16[2048,384]{1,0:T(8,128)(2,1)}) %all-gather.10.cloned.1.call-update) | async-done | bytes 1572880 | tf_op jit(solution)/shard_map/all_gather | solution.py:66
  213.5 3.1 fusion.72
  216.6 105.2 %all-gather.12.cloned.1.call-done = bf16[16384,256]{0,1:T(8,128)(2,1)} async-done(((bf16[256,256]{0,1:T(8,128)(2,1)}), bf16[16384,256]{0,1:T(8,128)(2,1)}) %all-gather.12.cloned.1.call-update) | async-done | bytes 8388624 | tf_op jit(solution)/shard_map/all_gather | solution.py:58
  321.8 5.8 %fusion.177 = (bf16[16384,128]{0,1:T(8,128)(2,1)}, bf16[16384,128]{0,1:T(8,128)(2,1)}) fusion(bf16[16384,256]{0,1:T(8,128)(2,1)} %all-gather.12.cloned.1.call-done), kind=kLoop, calls=%fused_computation.228 | loop fusion | bytes 16777216 | tf_op jit(solution)/shard_map/split | solution.py:59
  327.6 6.4 %copy.33 = bf16[16384,128]{1,0:T(8,128)(2,1)} copy(bf16[16384,128]{0,1:T(8,128)(2,1)} %get-tuple-element.367) | data formatting | bytes 8388608
  334.0 6.4 %copy.32 = bf16[16384,128]{1,0:T(8,128)(2,1)} copy(bf16[16384,128]{0,1:T(8,128)(2,1)} %get-tuple-element.368) | data formatting | bytes 8388608
  340.4 121.7 %while.28 = (s32[]{:T(128)}, f32[256,1,128]{0,2,1:T(8,128)S(1)}, f32[256,1]{0,1:T(1,128)S(1)}, s32[32]{0:T(128)S(1)}, s32[]{:T(128)}, /*index=5*/bf16[16384,128]...) while((s32[]{:T(128)}, f32[256,1,128]{0,2,1:T(8,128)S(1)}, ...), condition=%wide.region_8.9_spmd.clone, body=%wide.region_4.8_spmd.clone.sunk | while | flops 68059904 | bytes 1133913 | solution.py:275
  353.1 2.5 conditional.3
  356.9 2.5 conditional.3
  368.3 2.5 conditional.3
  372.1 2.5 conditional.3
  383.5 2.5 conditional.3
  464.5 20.0 %all_to_all.15 = bf16[8,32,2048]{2,1,0:T(8,128)(2,1)S(1)} all-to-all(bf16[8,32,2048]{2,1,0:T(8,128)(2,1)S(1)} %bitcast.298), channel_id=1, replica_groups=mesh['sp_0'=8,'sp_1'=8,'tp'=8] {'tp'}, dimensions={0} | all-to-all | bytes 2097152 | tf_op jit(solution)/shard_map/all_to_all | solution.py:83
  (360 shorter events, 193.8 us)
Async XLA Ops:
  6.5 23.5 %copy-start = (bf16[2048,256]{1,0:T(8,128)(2,1)S(1)}, bf16[2048,256]{1,0:T(8,128)(2,1)}, u32[]{:S(2)}) copy-start(bf16[2048,256]{1,0:T(8,128)(2,1)} %param.21) | copy-start | bytes 3145732
  9.8 20.2 %all-to-all-start = ((bf16[8,32,2048]{2,1,0:T(8,128)(2,1)}), bf16[8,32,2048]{2,1,0:T(8,128)(2,1)S(1)}, u32[]{:S(2)}, u32[]{:S(2)}) async-start(bf16[8,32,2048]{2,1,0:T(8,128)(2,1)} %broadcast_in_dim.28), calls=%async_computation | async-start | bytes 2097152 | tf_op jit(solution)/shard_map/all_to_all | solution.py:25
  14.1 66.8 %all-gather.14.cloned.1.call-start = ((), (), s32[]{:S(2)}) async-start(), calls=%async_computation.6 | async-start | bytes 2359296 | tf_op jit(solution)/shard_map/all_gather | solution.py:45
  30.0 2.2 copy-start.2
  41.3 0.7 copy-start.1
  41.3 39.6 %copy-start.6 = (f32[2,128,1,256]{1,0,3,2:T(2,128)}, f32[2,128,1,256]{1,0,3,2:T(2,128)S(1)}, u32[]{:S(2)}) copy-start(f32[2,128,1,256]{1,0,3,2:T(2,128)S(1)} %get-tuple-element.149) | copy-start | bytes 786436
  41.3 46.4 %copy-start.7 = (bf16[256,32]{0,1:T(8,128)(2,1)S(1)}, bf16[256,32]{0,1:T(8,128)(2,1)}, u32[]{:S(2)}) copy-start(bf16[256,32]{0,1:T(8,128)(2,1)} %param.26) | copy-start | bytes 49156
  41.3 47.8 %copy-start.3 = (bf16[2048,128]{1,0:T(8,128)(2,1)S(1)}, bf16[2048,128]{1,0:T(8,128)(2,1)}, u32[]{:S(2)}) copy-start(bf16[2048,128]{1,0:T(8,128)(2,1)} %param.24) | copy-start | bytes 1572868
  42.0 89.2 %all-gather.8.cloned.1.call-start = ((), (), s32[]{:S(2)}) async-start(), calls=%async_computation.3 | async-start | bytes 2359296 | tf_op jit(solution)/shard_map/all_gather | solution.py:45
  80.9 8.6 %copy-start.4 = (bf16[2048,128]{1,0:T(8,128)(2,1)S(1)}, bf16[2048,128]{1,0:T(8,128)(2,1)}, u32[]{:S(2)}) copy-start(bf16[2048,128]{1,0:T(8,128)(2,1)} %param.23) | copy-start | bytes 1572868
  87.6 125.9 %all-gather.10.cloned.1.call-start = ((), (), s32[]{:S(2)}) async-start(), calls=%async_computation.4 | async-start | bytes 1597440 | tf_op jit(solution)/shard_map/all_gather | solution.py:66
  89.0 232.8 %all-gather.12.cloned.1.call-start = ((), (), s32[]{:S(2)}) async-start(), calls=%async_computation.5 | async-start | bytes 8519680 | tf_op jit(solution)/shard_map/all_gather | solution.py:58
  89.6 39.5 %copy-start.5 = (bf16[2048,128]{1,0:T(8,128)(2,1)S(1)}, bf16[2048,128]{1,0:T(8,128)(2,1)}, u32[]{:S(2)}) copy-start(bf16[2048,128]{1,0:T(8,128)(2,1)} %param.22) | copy-start | bytes 1572868
  94.7 245.7 %all-to-all-start.1 = ((f32[64,256,1]{1,2,0:T(1,128)}), f32[64,256,1]{1,2,0:T(1,128)S(1)}, u32[]{:S(2)}, u32[]{:S(2)}) async-start(f32[64,256,1]{1,2,0:T(1,128)} %broadcast_in_dim.33), calls=%async_computation.1 | async-start | bytes 131072 | tf_op jit(solution)/shard_map/all_to_all | solution.py:25
  334.0 6.5 %copy-start.8 = (f32[256,1]{0,1:T(1,128)S(1)}, f32[256,1]{0,1:T(1,128)}, u32[]{:S(2)}) copy-start(f32[256,1]{0,1:T(1,128)} %param.25) | copy-start | bytes 3076
Sparse Core Ops, SparseCore 0:
  42.1 38.7 all-gather.13
  87.7 43.3 all-gather.7
  134.2 79.2 all-gather.9
  216.3 105.3 all-gather.11
where the time goes:
time: 494 us; the launch traced here: 492 us
  waiting for transfers between devices  214 us (43%)
  matrix products  98.6 us (20%)
  local copies, waits for them, and re-layouts  55.7 us (11%)
  blocking collectives  49.6 us (10%)
  loops' own time  23.7 us (5%)
  between operations  19.7 us (4%)
  starting transfers between devices  16.1 us (3%)
  other arithmetic  14.8 us (3%)
    all_gather x1, waiting for transfers between devices, side_by_side(): out = lax.all_gather(both, axis, axis=dim, tiled=True)  105 us
    all_gather x1, waiting for transfers between devices, rows_first(): out = lax.all_gather(both, axis, axis=0, tiled=True)  71 us
    dot_general x32, matrix products, fox_weights(): jnp.einsum('qhd,khd->hqk', queries, keys, preferred_element_type=jnp.floa...  39.5 us
    dot_general x32, matrix products, add_block(): jnp.einsum('hqk,khd->qhd', weights.astype(jnp.bfloat16), values, preferre...  36.7 us
    unnamed x2, blocking collectives  29.6 us
    another operation x1, loops' own time, per_device(): lax.scan(one_block, (zero_numer, zero_denom), jnp.arange(rows_here // wid...  22.1 us
    all_gather x2, waiting for transfers between devices, entering(): pieces = jax.tree.map(lambda part: lax.all_gather(part, axis), subtotal)  21.7 us
    all_to_all x1, blocking collectives, sent_and_summed(): pieces = lax.all_to_all(in_blocks(shard, dim, size), axis, 0, 0, tiled=True)  20 us
  transfers between devices with their start and end apart: 6, of which 5 were waited for; matrix products, arithmetic and copies ran while one was open for 9% of the time, Pallas kernels for 0%

commit v1 on v0

--- a/solution.py
+++ b/solution.py
@@ -63,7 +63,10 @@
     turned = [jnp.moveaxis(a, dim, 0) for a, dim in zip(arrays, dims)]
     widths = [t[0].size for t in turned]
     both = jnp.concatenate([t.reshape(-1, w) for t, w in zip(turned, widths)], axis=1)
-    out = lax.all_gather(both, axis, axis=0, tiled=True)
+    n_dev = lax.axis_size(axis)
+    shards = jnp.stack([both for _ in range(n_dev)])
+    shards = lax.all_to_all(shards, axis, split_axis=0, concat_axis=0)
+    out = jnp.concatenate(shards, axis=0)
     pieces = jnp.split(out, [sum(widths[:k]) for k in range(1, len(widths))], axis=1)
     return tuple(
         (

time: 494 us -> 441 us (0.89)
  waiting for transfers between devices: 214 us -> 125 us
  blocking collectives: 49.6 us -> 73.2 us
  starting transfers between devices: 16.1 us -> 27.6 us
    all_gather x1 -> x0, waiting for transfers between devices: 71 us -> none  [rows_first(): out = lax.all_gather(both, axis, axis=0, tiled=True)]
    all_gather x1, waiting for transfers between devices: 105 us -> 80.8 us  [side_by_side(): out = lax.all_gather(both, axis, axis=dim, tiled=True)]
    unnamed x2, blocking collectives: 29.6 us -> 53.2 us
    all_to_all x0 -> x1, starting transfers between devices: none -> 12 us  [rows_first(): shards = lax.all_to_all(shards, axis, split_axis=0, concat_axis=0)]
    all_gather x2, waiting for transfers between devices: 21.7 us -> 28.8 us  [entering(): pieces = jax.tree.map(lambda part: lax.all_gather(part, axis), subtotal)]
    unnamed x28 -> x32, local copies, waits for them, and re-layouts: 18.4 us -> 18.5 us
  transfers between devices with their start and end apart: 6 -> 6, of which waited for: 5 -> 4; matrix products, arithmetic and copies ran while one was open for 9% -> 10% of each run, Pallas kernels for 0% -> 0%
where the time goes in v1:
time: 441 us; the launch traced here: 438 us
  waiting for transfers between devices  125 us (28%)
  matrix products  99 us (22%)
  blocking collectives  73.2 us (17%)
  local copies, waits for them, and re-layouts  55.4 us (13%)
  starting transfers between devices  27.6 us (6%)
  loops' own time  23.7 us (5%)
  between operations  19.9 us (5%)
  other arithmetic  13.8 us (3%)
    all_gather x1, waiting for transfers between devices, side_by_side(): out = lax.all_gather(both, axis, axis=dim, tiled=True)  80.8 us
    unnamed x2, blocking collectives  53.2 us
    dot_general x32, matrix products, fox_weights(): jnp.einsum('qhd,khd->hqk', queries, keys, preferred_element_type=jnp.floa...  39.5 us
    dot_general x32, matrix products, add_block(): jnp.einsum('hqk,khd->qhd', weights.astype(jnp.bfloat16), values, preferre...  36.7 us
    all_gather x2, waiting for transfers between devices, entering(): pieces = jax.tree.map(lambda part: lax.all_gather(part, axis), subtotal)  28.8 us
    another operation x1, loops' own time, per_device(): lax.scan(one_block, (zero_numer, zero_denom), jnp.arange(rows_here // wid...  22.1 us
    all_to_all x1, blocking collectives, sent_and_summed(): pieces = lax.all_to_all(in_blocks(shard, dim, size), axis, 0, 0, tiled=True)  20 us
    dynamic_slice x32, local copies, waits for them, and re-layouts, per_device(): lax.scan(one_block, (zero_numer, zero_denom), jnp.arange(rows_here // wid...  18.8 us
  transfers between devices with their start and end apart: 6, of which 4 were waited for; matrix products, arithmetic and copies ran while one was open for 10% of the time, Pallas kernels for 0%

profile of v1, /device:TPU:496, one launch (start us, length us, event | category | flops | bytes accessed | tf_op | source)
XLA Modules:
  0.0 438.0 jit_solution(3140744757682495692)
XLA Ops:
  9.8 4.3 all-to-all-start
  14.3 15.7 %all-to-all-done = bf16[8,32,2048]{2,1,0:T(8,128)(2,1)S(1)} async-done(((bf16[8,32,2048]{2,1,0:T(8,128)(2,1)}), bf16[8,32,2048]{2,1,0:T(8,128)(2,1)S(1)}, u32[]{:S(2)}, u32[]{:S(2)}) %all-to-all-start) | async-done | bytes 1048608 | tf_op jit(solution)/shard_map/all_to_all | solution.py:25
  33.6 7.6 %while.29 = (s32[]{:T(128)}, f32[1,256,256]{2,1,0:T(8,128)S(1)}, f32[2,128,1,256]{1,0,3,2:T(2,128)S(1)}, f32[1]{0:T(128)}, bf16[2,128,1,256]{3,1,2,0:T(8,128)(2,...) while((s32[]{:T(128)}, f32[1,256,256]{2,1,0:T(8,128)S(1)}, ...), condition=%wide.region_2.3_spmd.clone.clone.clone, body=%wide.region_1.2_spmd.clone.clone.clone.sunk | while | flops 50872832 | bytes 1840267 | solution.py:166
  34.3 2.9 dynamic_update_slice.8
  38.1 2.9 dynamic_update_slice.8
  44.1 14.3 %all-reduce = f32[8]{0:T(128)S(1)} all-reduce(f32[8]{0:T(128)S(1)} %dynamic-update-slice), channel_id=2, replica_groups=mesh['sp_0'=8,'sp_1'=8,'tp'=8] {'sp_1'}, use_global_device_ids=true, to_apply=%add | all-reduce | flops 8 | bytes 64
  61.0 20.0 %all-gather.11.cloned.1.call-done = f32[8,256,256]{2,1,0:T(8,128)} async-done(((f32[1,256,256]{2,1,0:T(8,128)}), f32[8,256,256]{2,1,0:T(8,128)}) %all-gather.11.cloned.1.call-update) | async-done | bytes 2097168 | tf_op jit(solution)/shard_map/all_gather | solution.py:45
  81.0 6.8 %bitcast_add_fusion.4 = f32[1,1,256,256]{3,2,1,0:T(8,128)} fusion(f32[8,256,256]{2,1,0:T(8,128)} %all-gather.11.cloned.1.call-done, f32[]{:T(128)} %bitcast.32, f32[]{:T(128)} %bitcast.30, f32[]{:T(128)} %bitcast.28, f32[]{:T(128)} %bitcast.26, f32[]{:T(128)} %bitcast.24, f32[]{:T(128)} %bitcast.23, f32[]{:T(128)} %bitcast.22, f32[]{:T(128)} %bitcast.21), kind=kLoop, calls=%fused_computation.120 | loop fusion | flops 983040 | bytes 2359328 | tf_op jit(solution)/shard_map/add | solution.py:171
  91.0 12.0 %all-to-all-start.1 = ((bf16[64,32,384]{2,1,0:T(8,128)(2,1)}), bf16[64,32,384]{2,1,0:T(8,128)(2,1)}, u32[]{:S(2)}, u32[]{:S(2)}) async-start(bf16[64,32,384]{2,1,0:T(8,128)(2,1)} %stack.2), calls=%async_computation.1 | async-start | bytes 3145728 | tf_op jit(solution)/shard_map/all_to_all | solution.py:68
  105.7 38.9 %all-reduce.1 = f32[8]{0:T(128)S(1)} all-reduce(f32[8]{0:T(128)S(1)} %dynamic-update-slice.1), channel_id=3, replica_groups=mesh['sp_0'=8,'sp_1'=8,'tp'=8] {'sp_0'}, use_global_device_ids=true, to_apply=%add.1 | all-reduce | flops 8 | bytes 64
  151.6 8.8 %all-gather.7.cloned.1.call-done = f32[8,1,256,256]{3,2,1,0:T(8,128)} async-done(((f32[1,1,256,256]{3,2,1,0:T(8,128)}), f32[8,1,256,256]{3,2,1,0:T(8,128)}) %all-gather.7.cloned.1.call-update) | async-done | bytes 2097168 | tf_op jit(solution)/shard_map/all_gather | solution.py:45
  160.5 11.7 %multiply_reduce_fusion = (f32[256]{0:T(256)S(1)}, f32[256,1,256]{0,2,1:T(8,128)S(1)}) fusion(f32[256,1,256]{0,2,1:T(8,128)S(1)} %reshape.657, f32[256]{0:T(256)S(1)} %multiply_exponential_fusion, bf16[256,128]{0,1:T(8,128)(2,1)S(1)} %bitcast.301, bf16[256,128]{0,1:T(8,128)(2,1)S(1)} %bitcast.300, f32[8,1,256,256]{3,2,1,0:T(8,128)} %all-gather.7.cloned.1.call-done, ...), kind=kOutput, calls=%fused_computation.139 | convolution fusion | flops 37224192 | bytes 4851796 | tf_op jit(solution)/shard_map/thd,hde->the/dot_general | solution.py:246
  172.9 11.2 %all-to-all-start.2 = ((f32[64,256,1]{1,2,0:T(1,128)}), f32[64,256,1]{1,2,0:T(1,128)S(1)}, u32[]{:S(2)}, u32[]{:S(2)}) async-start(f32[64,256,1]{1,2,0:T(1,128)} %broadcast_in_dim.33), calls=%async_computation.2 | async-start | bytes 131072 | tf_op jit(solution)/shard_map/all_to_all | solution.py:25
  184.1 3.1 fusion.72
  187.2 80.8 %all-gather.9.cloned.1.call-done = bf16[16384,256]{0,1:T(8,128)(2,1)} async-done(((bf16[256,256]{0,1:T(8,128)(2,1)}), bf16[16384,256]{0,1:T(8,128)(2,1)}) %all-gather.9.cloned.1.call-update) | async-done | bytes 8388624 | tf_op jit(solution)/shard_map/all_gather | solution.py:58
  268.0 5.8 %fusion.177 = (bf16[16384,128]{0,1:T(8,128)(2,1)}, bf16[16384,128]{0,1:T(8,128)(2,1)}) fusion(bf16[16384,256]{0,1:T(8,128)(2,1)} %all-gather.9.cloned.1.call-done), kind=kLoop, calls=%fused_computation.228 | loop fusion | bytes 16777216 | tf_op jit(solution)/shard_map/split | solution.py:59
  273.8 6.4 %copy.33 = bf16[16384,128]{1,0:T(8,128)(2,1)} copy(bf16[16384,128]{0,1:T(8,128)(2,1)} %get-tuple-element.367) | data formatting | bytes 8388608
  280.2 6.4 %copy.32 = bf16[16384,128]{1,0:T(8,128)(2,1)} copy(bf16[16384,128]{0,1:T(8,128)(2,1)} %get-tuple-element.368) | data formatting | bytes 8388608
  286.6 121.7 %while.28 = (s32[]{:T(128)}, f32[256,1,128]{0,2,1:T(8,128)S(1)}, f32[256,1]{0,1:T(1,128)S(1)}, s32[32]{0:T(128)S(1)}, s32[]{:T(128)}, /*index=5*/bf16[16384,128]...) while((s32[]{:T(128)}, f32[256,1,128]{0,2,1:T(8,128)S(1)}, ...), condition=%wide.region_8.9_spmd.clone, body=%wide.region_4.8_spmd.clone.sunk | while | flops 68059904 | bytes 1133913 | solution.py:278
  295.5 2.5 conditional.3
  310.7 2.5 conditional.3
  314.5 2.5 conditional.3
  325.9 2.5 conditional.3
  410.7 20.0 %all_to_all.20 = bf16[8,32,2048]{2,1,0:T(8,128)(2,1)S(1)} all-to-all(bf16[8,32,2048]{2,1,0:T(8,128)(2,1)S(1)} %bitcast.299), channel_id=1, replica_groups=mesh['sp_0'=8,'sp_1'=8,'tp'=8] {'tp'}, dimensions={0} | all-to-all | bytes 2097152 | tf_op jit(solution)/shard_map/all_to_all | solution.py:86
  (364 shorter events, 193.1 us)
Async XLA Ops:
  6.5 23.5 %copy-start = (bf16[2048,256]{1,0:T(8,128)(2,1)S(1)}, bf16[2048,256]{1,0:T(8,128)(2,1)}, u32[]{:S(2)}) copy-start(bf16[2048,256]{1,0:T(8,128)(2,1)} %param.21) | copy-start | bytes 3145732
  9.8 20.2 %all-to-all-start = ((bf16[8,32,2048]{2,1,0:T(8,128)(2,1)}), bf16[8,32,2048]{2,1,0:T(8,128)(2,1)S(1)}, u32[]{:S(2)}, u32[]{:S(2)}) async-start(bf16[8,32,2048]{2,1,0:T(8,128)(2,1)} %broadcast_in_dim.28), calls=%async_computation | async-start | bytes 2097152 | tf_op jit(solution)/shard_map/all_to_all | solution.py:25
  14.1 66.9 %all-gather.11.cloned.1.call-start = ((), (), s32[]{:S(2)}) async-start(), calls=%async_computation.6 | async-start | bytes 2359296 | tf_op jit(solution)/shard_map/all_gather | solution.py:45
  30.0 2.2 copy-start.2
  41.2 0.7 copy-start.1
  41.3 39.7 %copy-start.6 = (f32[2,128,1,256]{1,0,3,2:T(2,128)}, f32[2,128,1,256]{1,0,3,2:T(2,128)S(1)}, u32[]{:S(2)}) copy-start(f32[2,128,1,256]{1,0,3,2:T(2,128)S(1)} %get-tuple-element.149) | copy-start | bytes 786436
  41.3 46.6 %copy-start.3 = (bf16[2048,128]{1,0:T(8,128)(2,1)S(1)}, bf16[2048,128]{1,0:T(8,128)(2,1)}, u32[]{:S(2)}) copy-start(bf16[2048,128]{1,0:T(8,128)(2,1)} %param.24) | copy-start | bytes 1572868
  42.0 118.5 %all-gather.7.cloned.1.call-start = ((), (), s32[]{:S(2)}) async-start(), calls=%async_computation.4 | async-start | bytes 2359296 | tf_op jit(solution)/shard_map/all_gather | solution.py:45
  81.0 7.4 %copy-start.4 = (bf16[2048,128]{1,0:T(8,128)(2,1)S(1)}, bf16[2048,128]{1,0:T(8,128)(2,1)}, u32[]{:S(2)}) copy-start(bf16[2048,128]{1,0:T(8,128)(2,1)} %param.23) | copy-start | bytes 1572868
  87.8 1.8 copy-start.8
  87.8 1.8 copy-start.9
  87.9 180.1 %all-gather.9.cloned.1.call-start = ((), (), s32[]{:S(2)}) async-start(), calls=%async_computation.5 | async-start | bytes 8519680 | tf_op jit(solution)/shard_map/all_gather | solution.py:58
  89.6 61.3 %copy-start.7 = (f32[2,128,1,256]{1,0,3,2:T(2,128)S(1)}, f32[2,128,1,256]{1,0,3,2:T(2,128)}, u32[]{:S(2)}) copy-start(f32[2,128,1,256]{1,0,3,2:T(2,128)} %copy-done.6) | copy-start | bytes 786436
  90.9 60.2 %copy-start.5 = (bf16[2048,128]{1,0:T(8,128)(2,1)S(1)}, bf16[2048,128]{1,0:T(8,128)(2,1)}, u32[]{:S(2)}) copy-start(bf16[2048,128]{1,0:T(8,128)(2,1)} %param.22) | copy-start | bytes 1572868
  91.0 81.3 %all-to-all-start.1 = ((bf16[64,32,384]{2,1,0:T(8,128)(2,1)}), bf16[64,32,384]{2,1,0:T(8,128)(2,1)}, u32[]{:S(2)}, u32[]{:S(2)}) async-start(bf16[64,32,384]{2,1,0:T(8,128)(2,1)} %stack.2), calls=%async_computation.1 | async-start | bytes 3145728 | tf_op jit(solution)/shard_map/all_to_all | solution.py:68
  160.5 11.8 %copy-start.10 = (f32[256,1]{0,1:T(1,128)S(1)}, f32[256,1]{0,1:T(1,128)}, u32[]{:S(2)}) copy-start(f32[256,1]{0,1:T(1,128)} %param.25) | copy-start | bytes 3076
  172.9 113.7 %all-to-all-start.2 = ((f32[64,256,1]{1,2,0:T(1,128)}), f32[64,256,1]{1,2,0:T(1,128)S(1)}, u32[]{:S(2)}, u32[]{:S(2)}) async-start(f32[64,256,1]{1,2,0:T(1,128)} %broadcast_in_dim.33), calls=%async_computation.2 | async-start | bytes 131072 | tf_op jit(solution)/shard_map/all_to_all | solution.py:25
Sparse Core Ops, SparseCore 0:
  42.1 38.8 all-gather.10
  88.0 72.4 all-gather.6
  163.5 104.4 all-gather.8
